TPU v7x, 32 devices: a whole 2x2x4 slice. The times are simulated.
32 devices in a mesh: sp: 8 (over z, x), tp: 4 (over y, core).
Axes of the slice: x: 2, y: 2, z: 4, core: 2. Of those that a mesh axis runs over, the one named last changes fastest.
Arguments:
- cotangent: bfloat16 [1024, 2048], P('sp'), may hold values from -6 to 6
- stream: bfloat16 [1024, 2048], P('sp'), may hold values from -6 to 6
- routes: int32 [1024, 2], P('sp'), may hold values from 0 to 3, all different within a row; in each aligned block of 128 rows (0 to 127, 128 to 255, ...) at most 96 rows name the same one
- route_weights: float32 [1024, 2], P('sp'), may hold values from 0.25 to 1
- gate_weight: bfloat16 [8, 2048, 2048], P('sp', None, 'tp'), may hold values from -0.125 to 0.125
- up_weight: bfloat16 [8, 2048, 2048], P('sp', None, 'tp'), may hold values from -0.125 to 0.125
- down_weight: bfloat16 [8, 2048, 2048], P('sp', 'tp'), may hold values from -0.09375 to 0.09375
- outer_gate: bfloat16 [1024, 1024], P('sp', 'tp'), may hold values from -6 to 6
- inner_gate: bfloat16 [1024, 1024], P('sp', 'tp'), may hold values from -6 to 6
- conv_input: bfloat16 [1024, 1024], P('sp', 'tp'), may hold values from -6 to 6
- conv_taps: bfloat16 [3, 1024], P(None, 'tp'), may hold values from -1 to 1
- out_weight: bfloat16 [2048, 1024], P(None, 'tp'), may hold values from -0.1875 to 0.1875
Outputs:
- gate_grad: bfloat16 [8, 2048, 2048], P('sp', None, 'tp')
- up_grad: bfloat16 [8, 2048, 2048], P('sp', None, 'tp')
- down_grad: bfloat16 [8, 2048, 2048], P('sp', 'tp')
- out_grad: float32 [2048, 1024], P('sp', 'tp')
- outer_grad: bfloat16 [1024, 1024], P('sp', 'tp')
- inner_grad: bfloat16 [1024, 1024], P('sp', 'tp')
- input_grad: bfloat16 [1024, 1024], P('sp', 'tp')
Inputs may be any that keep to these rules, and one draw needn't show every extreme that they name: `routes`: each token names two different experts. Among the 128 tokens of one index of sp no expert is named by more than 96 tokens, a bound that some block of them reaches in every draw.
All inputs are finite; a program needn't handle non-finite values.
Results may differ from a plain program's by a relative error of at most 0.02.
Values may be sent and summed in bfloat16 or wider, within the bound.
A program may use at most 64 MiB of HBM per device.

v0:
```python
import jax
import jax.numpy as jnp
from jax import lax
from jax.sharding import PartitionSpec as P


def from_behind(block, axis, distance):
    devices = range(lax.axis_size(axis))
    route = [(i - distance, i) for i in devices if i - distance in devices]
    return lax.ppermute(block, axis, route)


def per_device(
    cotangent,
    stream,
    routes,
    route_weights,
    gate_weight,
    up_weight,
    down_weight,
    outer_gate,
    inner_gate,
    conv_input,
    conv_taps,
    out_weight,
):
    groups = lax.axis_size("sp")
    tp_count = lax.axis_size("tp")
    experts = groups // 2
    tok_rows = stream.shape[0]
    model_width = stream.shape[1]
    capacity = 3 * tok_rows // experts
    slot_total = experts * capacity
    contract_first = (((0,), (0,)), ((), ()))
    contract_last = (((1,), (1,)), ((), ()))
    flat_routes = routes.reshape(-1)
    choose = (flat_routes[:, None] == jnp.arange(experts, dtype=jnp.int32)[None, :]).astype(
        jnp.int32
    )
    before = jnp.cumsum(choose, axis=0) - choose
    slot_place = flat_routes * capacity + jnp.sum(before * choose, axis=1)
    slot_table = (jnp.arange(slot_total, dtype=jnp.int32)[:, None] == slot_place[None, :]).astype(
        jnp.float32
    )
    select = jnp.sum(slot_table.reshape(slot_total, tok_rows, 2), axis=2).astype(jnp.bfloat16)
    slot_weight = jnp.sum(slot_table * route_weights.reshape(-1)[None, :], axis=1)
    block_width = model_width // tp_count
    offset = lax.axis_index("tp") * block_width
    rows_part = lax.dynamic_slice_in_dim(stream, offset, block_width, 1)
    cot_part = lax.dynamic_slice_in_dim(cotangent, offset, block_width, 1)
    sent_rows = jnp.dot(select, rows_part, preferred_element_type=jnp.float32).astype(jnp.bfloat16)
    sent_cot = (
        jnp.dot(select, cot_part, preferred_element_type=jnp.float32) * slot_weight[:, None]
    ).astype(jnp.bfloat16)
    sent_rows = jnp.repeat(sent_rows.reshape(experts, capacity, -1), 2, axis=0)
    sent_cot = jnp.repeat(sent_cot.reshape(experts, capacity, -1), 2, axis=0)
    recv_rows, recv_cot = (
        lax.all_to_all(sent_rows, "sp", split_axis=0, concat_axis=0, tiled=True),
        lax.all_to_all(sent_cot, "sp", split_axis=0, concat_axis=0, tiled=True),
    )
    recv_rows, recv_cot = (
        lax.all_gather(recv_rows, "tp", axis=2, tiled=True),
        lax.all_gather(recv_cot, "tp", axis=2, tiled=True),
    )
    slots = groups * capacity
    routed_rows = recv_rows.reshape(slots, model_width)
    routed_cot = recv_cot.reshape(slots, model_width)
    gate_local = gate_weight[0]
    up_local = up_weight[0]
    down_local = down_weight[0]
    gate_pre = jnp.dot(routed_rows, gate_local, preferred_element_type=jnp.float32)
    up_pre = jnp.dot(routed_rows, up_local, preferred_element_type=jnp.float32)
    hidden_grad = lax.dot_general(
        routed_cot, down_local, contract_last, preferred_element_type=jnp.float32
    )
    sigma = jax.nn.sigmoid(gate_pre)
    silu_gate = gate_pre * sigma
    hidden = (silu_gate * up_pre).astype(jnp.bfloat16)
    up_delta = (hidden_grad * silu_gate).astype(jnp.bfloat16)
    gate_delta = (hidden_grad * up_pre * sigma * (1.0 + gate_pre * (1.0 - sigma))).astype(
        jnp.bfloat16
    )
    gate_grad = lax.dot_general(
        routed_rows, gate_delta, contract_first, preferred_element_type=jnp.float32
    ).astype(jnp.bfloat16)[None]
    up_grad = lax.dot_general(
        routed_rows, up_delta, contract_first, preferred_element_type=jnp.float32
    ).astype(jnp.bfloat16)[None]
    down_grad = lax.dot_general(
        hidden, routed_cot, contract_first, preferred_element_type=jnp.float32
    ).astype(jnp.bfloat16)[None]
    row_partial = lax.dot_general(
        gate_delta, gate_local, contract_last, preferred_element_type=jnp.float32
    )
    row_partial = row_partial + lax.dot_general(
        up_delta, up_local, contract_last, preferred_element_type=jnp.float32
    )
    half_sums = lax.psum_scatter(
        row_partial.astype(jnp.bfloat16), "tp", scatter_dimension=1, tiled=True
    ).astype(jnp.float32)
    block_width = half_sums.shape[1]
    half_grad = half_sums.reshape(groups, capacity, block_width).astype(jnp.bfloat16)
    returned = lax.all_to_all(half_grad, "sp", split_axis=0, concat_axis=0, tiled=True)
    returned = returned.reshape(experts, 2, capacity, block_width)
    select_three = select.reshape(experts, capacity, tok_rows)
    moe_part = jnp.einsum(
        "ecr,emcd->rd", select_three, returned, preferred_element_type=jnp.float32
    ).astype(jnp.bfloat16)
    moe_grad = lax.all_gather(moe_part, "tp", axis=1, tiled=True)
    stream_grad = (cotangent.astype(jnp.float32) + moe_grad.astype(jnp.float32)).astype(
        jnp.bfloat16
    )
    taps = conv_taps.astype(jnp.float32)
    outer_f = outer_gate.astype(jnp.float32)
    inner_f = inner_gate.astype(jnp.float32)
    input_f = conv_input.astype(jnp.float32)
    mixed = inner_f * input_f
    earlier = from_behind(mixed[-2:], "sp", 1)
    padded = jnp.concatenate([earlier, mixed], axis=0)
    conv_sum = taps[0] * padded[:-2] + taps[1] * padded[1:-1] + taps[2] * padded[2:]
    conv_out = (outer_f * conv_sum).astype(jnp.bfloat16)
    out_grad = lax.psum_scatter(
        lax.dot_general(
            stream_grad, conv_out, contract_first, preferred_element_type=jnp.float32
        ).astype(jnp.bfloat16),
        "sp",
        scatter_dimension=0,
        tiled=True,
    ).astype(jnp.float32)
    conv_grad = jnp.dot(stream_grad, out_weight, preferred_element_type=jnp.float32)
    outer_grad = (conv_grad * conv_sum).astype(jnp.bfloat16)
    scaled = conv_grad * outer_f
    later = from_behind(scaled[:2], "sp", -1)
    extended = jnp.concatenate([scaled, later], axis=0)
    mixed_grad = taps[2] * extended[:-2] + taps[1] * extended[1:-1] + taps[0] * extended[2:]
    inner_grad = (mixed_grad * input_f).astype(jnp.bfloat16)
    input_grad = (mixed_grad * inner_f).astype(jnp.bfloat16)
    return (gate_grad, up_grad, down_grad, out_grad, outer_grad, inner_grad, input_grad)


def solution(mesh):
    placed = (
        P("sp", None),
        P("sp", None),
        P("sp", None),
        P("sp", None),
        P("sp", None, "tp"),
        P("sp", None, "tp"),
        P("sp", "tp", None),
        P("sp", "tp"),
        P("sp", "tp"),
        P("sp", "tp"),
        P(None, "tp"),
        P(None, "tp"),
    )
    return jax.shard_map(
        per_device,
        mesh=mesh,
        in_specs=placed,
        out_specs=(
            P("sp", None, "tp"),
            P("sp", None, "tp"),
            P("sp", "tp", None),
            P("sp", "tp"),
            P("sp", "tp"),
            P("sp", "tp"),
            P("sp", "tp"),
        ),
        check_vma=False,
    )
```

profile of v0, /device:TPU:0, one launch (start us, length us, event | category | flops | bytes accessed | tf_op | source)
XLA Modules:
  0.0 253.2 jit_solution(881290032400397519)
XLA Ops:
  8.5 1.2 reduce-window.6
  11.1 1.2 convolution_convert_fusion.4
  12.4 27.3 %all_to_all.15 = bf16[8,96,512]{2,1,0:T(8,128)(2,1)} all-to-all(bf16[8,96,512]{2,1,0:T(8,128)(2,1)S(1)} %bitcast.73), channel_id=1, replica_groups=mesh['sp'=8,'tp'=4] {'sp'}, dimensions={0} | all-to-all | bytes 1572864 | tf_op jit(solution)/shard_map/all_to_all | solution.py:58
  40.6 23.3 %all_to_all.16 = bf16[8,96,512]{2,1,0:T(8,128)(2,1)} all-to-all(bf16[8,96,512]{2,1,0:T(8,128)(2,1)S(1)} %bitcast.74), channel_id=1, replica_groups=mesh['sp'=8,'tp'=4] {'sp'}, dimensions={0} | all-to-all | bytes 1572864 | tf_op jit(solution)/shard_map/all_to_all | solution.py:59
  63.9 3.5 %all-gather.3.cloned.1.call-done = bf16[8,96,2048]{2,1,0:T(8,128)(2,1)} async-done(((bf16[8,96,512]{2,1,0:T(8,128)(2,1)}), bf16[8,96,2048]{2,1,0:T(8,128)(2,1)}) %all-gather.3.cloned.1.call-update) | async-done | bytes 3145744 | tf_op jit(solution)/shard_map/all_gather | solution.py:62
  67.4 5.0 %fusion.5 = f32[768,512]{1,0:T(8,128)} fusion(bf16[768,2048]{1,0:T(8,128)(2,1)} %bitcast.86, bf16[1,2048,512]{2,1,0:T(8,128)(2,1)S(1)} %copy-done), kind=kOutput, calls=%fused_computation.10 | convolution fusion | flops 1610612736 | bytes 6815744 | tf_op jit(solution)/shard_map/dot_general | solution.py:71
  72.4 2.9 %fusion.8 = f32[768,512]{1,0:T(8,128)} fusion(bf16[768,2048]{1,0:T(8,128)(2,1)S(1)} %bitcast.88, bf16[1,2048,512]{2,1,0:T(8,128)(2,1)S(1)} %copy-done.2), kind=kOutput, calls=%fused_computation.13 | convolution fusion | flops 1610612736 | bytes 6815744 | tf_op jit(solution)/shard_map/dot_general | solution.py:72
  75.3 22.2 %all-gather.5.cloned.1.call-done = bf16[8,96,2048]{2,1,0:T(8,128)(2,1)} async-done(((bf16[8,96,512]{2,1,0:T(8,128)(2,1)}), bf16[8,96,2048]{2,1,0:T(8,128)(2,1)}) %all-gather.5.cloned.1.call-update) | async-done | bytes 3145744 | tf_op jit(solution)/shard_map/all_gather | solution.py:63
  97.5 5.7 %multiply_convert_fusion.1 = (bf16[768,512]{1,0:T(8,128)(2,1)S(1)}, bf16[768,512]{1,0:T(8,128)(2,1)S(1)}) fusion(f32[768,512]{1,0:T(8,128)} %fusion.5, f32[768,512]{1,0:T(8,128)} %fusion.8, bf16[768,2048]{1,0:T(8,128)(2,1)} %bitcast.90, bf16[1,512,2048]{2,1,0:T(8,128)(2,1)} %param.18), kind=kOutput, calls=%fused_computation.19 | convolution fusion | flops 1615724544 | bytes 9961472 | tf_op jit(solution)/shard_map/dot_general | solution.py:73
  103.3 1.8 fusion.3
  105.4 3.5 %add_convert_fusion = bf16[768,2048]{1,0:T(8,128)(2,1)} fusion(f32[768,2048]{1,0:T(8,128)S(1)} %fusion.3, bf16[768,512]{1,0:T(8,128)(2,1)S(1)} %get-tuple-element.11, bf16[1,2048,512]{2,1,0:T(8,128)(2,1)S(1)} %copy-done.3), kind=kOutput, calls=%fused_computation | convolution fusion | flops 1613758464 | bytes 12320768 | tf_op jit(solution)/shard_map/dot_general | solution.py:95
  109.0 37.9 %reduce-scatter.3.cloned.1.call-done = bf16[768,512]{1,0:T(8,128)(2,1)} async-done(((bf16[768,2048]{1,0:T(8,128)(2,1)}), bf16[768,512]{1,0:T(8,128)(2,1)}) %reduce-scatter.3.cloned.1.call-update) | async-done | bytes 786448 | tf_op jit(solution)/shard_map/reduce_scatter | solution.py:98
  146.8 5.5 %all-to-all-start.2 = ((bf16[8,96,512]{2,1,0:T(8,128)(2,1)}), bf16[8,96,512]{2,1,0:T(8,128)(2,1)S(1)}, u32[]{:S(2)}, u32[]{:S(2)}) async-start(bf16[8,96,512]{2,1,0:T(8,128)(2,1)} %bitcast.78), calls=%async_computation.3 | async-start | bytes 1572864 | tf_op jit(solution)/shard_map/all_to_all | solution.py:103
  153.3 3.9 %collective-permute-start = (f32[2,256]{1,0:T(2,128)S(1)}, f32[2,256]{1,0:T(2,128)S(1)}, u32[]{:S(2)}, u32[]{:S(2)}) collective-permute-start(f32[2,256]{1,0:T(2,128)S(1)} %slice.49), channel_id=1, source_target_pairs={{0,4},{4,8},{8,12},{12,16},{16,20},{20,24},{24,28},{1,5},{5,9},{9,... | collective-permute-start | bytes 6152 | tf_op jit(solution)/shard_map/ppermute | solution.py:10
  157.2 15.2 %all-to-all-done.2 = bf16[8,96,512]{2,1,0:T(8,128)(2,1)S(1)} async-done(((bf16[8,96,512]{2,1,0:T(8,128)(2,1)}), bf16[8,96,512]{2,1,0:T(8,128)(2,1)S(1)}, u32[]{:S(2)}, u32[]{:S(2)}) %all-to-all-start.2) | async-done | bytes 786464 | tf_op jit(solution)/shard_map/all_to_all | solution.py:103
  172.8 6.7 %all_gather.11 = bf16[128,2048]{1,0:T(8,128)(2,1)S(1)} all-gather(bf16[128,512]{1,0:T(8,128)(2,1)S(1)} %fusion.14), channel_id=1, replica_groups=mesh['sp'=8,'tp'=4] {'tp'}, dimensions={1}, use_global_device_ids=true | all-gather | bytes 655360 | tf_op jit(solution)/shard_map/all_gather | solution.py:109
  179.5 1.0 multiply_convert_fusion.4
  180.5 1.5 convolution_convert_fusion.3
  182.1 5.2 %fusion = bf16[1,2048,512]{2,1,0:T(8,128)(2,1)} fusion(bf16[768,2048]{1,0:T(8,128)(2,1)} %bitcast.87, bf16[768,512]{1,0:T(8,128)(2,1)S(1)} %copy-done.8), kind=kOutput, calls=%fused_computation.4 | convolution fusion | flops 1611661312 | bytes 6029312 | tf_op jit(solution)/shard_map/dot_general | solution.py:83
  187.3 3.3 %fusion.2 = bf16[1,512,2048]{2,1,0:T(8,128)(2,1)} fusion(bf16[768,2048]{1,0:T(8,128)(2,1)S(1)} %bitcast.91, f32[768,512]{1,0:T(8,128)S(1)} %copy-done.21, f32[768,512]{1,0:T(8,128)S(1)} %copy-done.20), kind=kOutput, calls=%fused_computation.6 | convolution fusion | flops 1614020608 | bytes 8388608 | tf_op jit(solution)/shard_map/dot_general | solution.py:89
  190.6 1.4 collective-permute-start.1
  192.1 3.2 %fusion.1 = bf16[1,2048,512]{2,1,0:T(8,128)(2,1)} fusion(bf16[768,2048]{1,0:T(8,128)(2,1)S(1)} %bitcast.89, bf16[768,512]{1,0:T(8,128)(2,1)S(1)} %copy-done.6), kind=kOutput, calls=%fused_computation.5 | convolution fusion | flops 1611661312 | bytes 6029312 | tf_op jit(solution)/shard_map/dot_general | solution.py:86
  197.6 47.4 %reduce-scatter.5.cloned.1.call-done = bf16[256,256]{1,0:T(8,128)(2,1)} async-done(((bf16[2048,256]{1,0:T(8,128)(2,1)}), bf16[256,256]{1,0:T(8,128)(2,1)}) %reduce-scatter.5.cloned.1.call-update) | async-done | bytes 131088 | tf_op jit(solution)/shard_map/reduce_scatter | solution.py:122
  245.0 1.6 convert_element_type.125
  (84 shorter events, 7.6 us)
Async XLA Ops:
  7.2 60.3 %copy-start = (bf16[1,2048,512]{2,1,0:T(8,128)(2,1)S(1)}, bf16[1,2048,512]{2,1,0:T(8,128)(2,1)}, u32[]{:S(2)}) copy-start(bf16[1,2048,512]{2,1,0:T(8,128)(2,1)} %param.16) | copy-start | bytes 6291460
  7.2 60.3 %all-gather.3.cloned.1.call-start = ((), (), s32[]{:S(2)}) async-start(), calls=%async_computation.5 | async-start | bytes 3932160 | tf_op jit(solution)/shard_map/all_gather | solution.py:62
  11.1 28.7 %copy-start.16 = (f32[128,2]{0,1:T(2,128)S(1)}, f32[128,2]{0,1:T(2,128)}, u32[]{:S(2)}) copy-start(f32[128,2]{0,1:T(2,128)} %param.15) | copy-start | bytes 3076
  11.1 29.1 %copy-start.1 = (bf16[128,2048]{1,0:T(8,128)(2,1)S(1)}, bf16[128,2048]{1,0:T(8,128)(2,1)}, u32[]{:S(2)}) copy-start(bf16[128,2048]{1,0:T(8,128)(2,1)} %param.12) | copy-start | bytes 1572868
  39.7 57.8 %all-gather.5.cloned.1.call-start = ((), (), s32[]{:S(2)}) async-start(), calls=%async_computation.6 | async-start | bytes 3932160 | tf_op jit(solution)/shard_map/all_gather | solution.py:63
  63.9 83.0 %reduce-scatter.3.cloned.1.call-start = ((), (), s32[]{:S(2)}) async-start(), calls=%async_computation.7 | async-start | bytes 3932160 | tf_op jit(solution)/shard_map/reduce_scatter | solution.py:98
  67.4 5.0 %copy-start.2 = (bf16[1,2048,512]{2,1,0:T(8,128)(2,1)S(1)}, bf16[1,2048,512]{2,1,0:T(8,128)(2,1)}, u32[]{:S(2)}) copy-start(bf16[1,2048,512]{2,1,0:T(8,128)(2,1)} %param.17) | copy-start | bytes 6291460
  67.4 5.0 %copy-start.17 = (bf16[8,96,2048]{2,1,0:T(8,128)(2,1)S(1)}, bf16[8,96,2048]{2,1,0:T(8,128)(2,1)}, u32[]{:S(2)}) copy-start(bf16[8,96,2048]{2,1,0:T(8,128)(2,1)} %all-gather.3.cloned.1.call-done) | copy-start | bytes 9437188
  108.9 48.3 %copy-start.15 = (bf16[3,256]{1,0:T(4,128)(2,1)S(1)}, bf16[3,256]{1,0:T(4,128)(2,1)}, u32[]{:S(2)}) copy-start(bf16[3,256]{1,0:T(4,128)(2,1)} %param.22) | copy-start | bytes 4612
  146.8 25.6 %all-to-all-start.2 = ((bf16[8,96,512]{2,1,0:T(8,128)(2,1)}), bf16[8,96,512]{2,1,0:T(8,128)(2,1)S(1)}, u32[]{:S(2)}, u32[]{:S(2)}) async-start(bf16[8,96,512]{2,1,0:T(8,128)(2,1)} %bitcast.78), calls=%async_computation.3 | async-start | bytes 1572864 | tf_op jit(solution)/shard_map/all_to_all | solution.py:103
  152.4 92.7 %reduce-scatter.5.cloned.1.call-start = ((), (), s32[]{:S(2)}) async-start(), calls=%async_computation.8 | async-start | bytes 1179648 | tf_op jit(solution)/shard_map/reduce_scatter | solution.py:122
  153.3 3.9 %copy-start.10 = (f32[128,256]{1,0:T(8,128)}, f32[128,256]{1,0:T(8,128)S(1)}, u32[]{:S(2)}) copy-start(f32[128,256]{1,0:T(8,128)S(1)} %convert_multiply_fusion.1) | copy-start | bytes 393220
  153.3 26.2 %collective-permute-start = (f32[2,256]{1,0:T(2,128)S(1)}, f32[2,256]{1,0:T(2,128)S(1)}, u32[]{:S(2)}, u32[]{:S(2)}) collective-permute-start(f32[2,256]{1,0:T(2,128)S(1)} %slice.49), channel_id=1, source_target_pairs={{0,4},{4,8},{8,12},{12,16},{16,20},{20,24},{24,28},{1,5},{5,9},{9,... | collective-permute-start | bytes 6152 | tf_op jit(solution)/shard_map/ppermute | solution.py:10
  172.4 7.1 %copy-start.4 = (bf16[2048,256]{1,0:T(8,128)(2,1)S(1)}, bf16[2048,256]{1,0:T(8,128)(2,1)}, u32[]{:S(2)}) copy-start(bf16[2048,256]{1,0:T(8,128)(2,1)} %param.23) | copy-start | bytes 3145732
  172.4 7.1 %copy-start.11 = (f32[128,256]{1,0:T(8,128)S(1)}, f32[128,256]{1,0:T(8,128)}, u32[]{:S(2)}) copy-start(f32[128,256]{1,0:T(8,128)} %copy-done.10) | copy-start | bytes 393220
  172.4 7.1 %copy-start.12 = (bf16[128,256]{1,0:T(8,128)(2,1)S(1)}, bf16[128,256]{1,0:T(8,128)(2,1)}, u32[]{:S(2)}) copy-start(bf16[128,256]{1,0:T(8,128)(2,1)} %param.19) | copy-start | bytes 196612
  182.0 5.2 %copy-start.19 = (bf16[8,96,2048]{2,1,0:T(8,128)(2,1)S(1)}, bf16[8,96,2048]{2,1,0:T(8,128)(2,1)}, u32[]{:S(2)}) copy-start(bf16[8,96,2048]{2,1,0:T(8,128)(2,1)} %all-gather.5.cloned.1.call-done) | copy-start | bytes 9437188
  182.0 5.2 %copy-start.20 = (f32[768,512]{1,0:T(8,128)S(1)}, f32[768,512]{1,0:T(8,128)}, u32[]{:S(2)}) copy-start(f32[768,512]{1,0:T(8,128)} %fusion.5) | copy-start | bytes 4718596
  182.1 5.2 %copy-start.21 = (f32[768,512]{1,0:T(8,128)S(1)}, f32[768,512]{1,0:T(8,128)}, u32[]{:S(2)}) copy-start(f32[768,512]{1,0:T(8,128)} %fusion.8) | copy-start | bytes 4718596
  187.3 4.8 %copy-start.6 = (bf16[768,512]{1,0:T(8,128)(2,1)S(1)}, bf16[768,512]{1,0:T(8,128)(2,1)}, u32[]{:S(2)}) copy-start(bf16[768,512]{1,0:T(8,128)(2,1)} %copy-done.5) | copy-start | bytes 2359300
  187.3 4.8 %copy-start.18 = (bf16[8,96,2048]{2,1,0:T(8,128)(2,1)S(1)}, bf16[8,96,2048]{2,1,0:T(8,128)(2,1)}, u32[]{:S(2)}) copy-start(bf16[8,96,2048]{2,1,0:T(8,128)(2,1)} %all-gather.3.cloned.1.call-done) | copy-start | bytes 9437188
  190.6 5.6 %copy-start.13 = (bf16[128,256]{1,0:T(8,128)(2,1)S(1)}, bf16[128,256]{1,0:T(8,128)(2,1)}, u32[]{:S(2)}) copy-start(bf16[128,256]{1,0:T(8,128)(2,1)} %param.20) | copy-start | bytes 196612
  190.6 6.3 %copy-start.14 = (bf16[128,256]{1,0:T(8,128)(2,1)S(1)}, bf16[128,256]{1,0:T(8,128)(2,1)}, u32[]{:S(2)}) copy-start(bf16[128,256]{1,0:T(8,128)(2,1)} %param.21) | copy-start | bytes 196612
  190.6 5.6 %collective-permute-start.1 = (f32[2,256]{1,0:T(2,128)S(1)}, f32[2,256]{1,0:T(2,128)S(1)}, u32[]{:S(2)}, u32[]{:S(2)}) collective-permute-start(f32[2,256]{1,0:T(2,128)S(1)} %slice.54), channel_id=1, source_target_pairs={{4,0},{8,4},{12,8},{16,12},{20,16},{24,20},{28,24},{5,1},{9,5},{13... | collective-permute-start | bytes 6152 | tf_op jit(solution)/shard_map/ppermute | solution.py:10
  (5 other events, 10.8 us)
Sparse Core Ops, SparseCore 0:
  39.9 27.5 all-gather.2
  69.0 28.4 all-gather.4
  109.1 37.7 reduce-scatter.2
  182.1 62.8 reduce-scatter.4
where the time goes:
time: 254 us; the launch traced here: 253 us
  waiting for transfers between devices  127 us (50%)
  blocking collectives  57.3 us (23%)
  matrix products  34.8 us (14%)
  between operations  14.1 us (6%)
  starting transfers between devices  11 us (4%)
  other arithmetic  6.23 us (2%)
    reduce_scatter x1, waiting for transfers between devices, per_device(): lax.psum_scatter(lax.dot_general(stream_grad, conv_out, contract_first, p...  47.4 us
    reduce_scatter x1, waiting for transfers between devices, per_device(): lax.psum_scatter(row_partial.astype(jnp.bfloat16), 'tp', scatter_dimensio...  37.9 us
    all_to_all x1, blocking collectives, per_device(): lax.all_to_all(sent_rows, 'sp', split_axis=0, concat_axis=0, tiled=True)  27.3 us
    all_to_all x1, blocking collectives, per_device(): lax.all_to_all(sent_cot, 'sp', split_axis=0, concat_axis=0, tiled=True)  23.3 us
    all_gather x1, waiting for transfers between devices, per_device(): lax.all_gather(recv_cot, 'tp', axis=2, tiled=True)  22.2 us
    all_to_all x1, waiting for transfers between devices, per_device(): lax.all_to_all(half_grad, 'sp', split_axis=0, concat_axis=0, tiled=True)  15.2 us
    all_gather x1, blocking collectives, per_device(): moe_grad = lax.all_gather(moe_part, 'tp', axis=1, tiled=True)  6.68 us
    dot_general x1, matrix products, per_device(): lax.dot_general(routed_cot, down_local, contract_last, preferred_element_...  5.69 us
  transfers between devices with their start and end apart: 7, of which 6 were waited for; matrix products, arithmetic and copies ran while one was open for 9% of the time, Pallas kernels for 0%

commit v1 on v0

--- a/solution.py
+++ b/solution.py
@@ -2,6 +2,23 @@
 import jax.numpy as jnp
 from jax import lax
 from jax.sharding import PartitionSpec as P
+
+
+def joined_along(blocks, dim):
+    blocks = jnp.moveaxis(blocks, 0, dim)
+    lengths = blocks.shape
+    return blocks.reshape(*lengths[:dim], lengths[dim] * lengths[dim + 1], *lengths[dim + 2 :])
+
+
+def ring_gather(x, axis, dim):
+    devices = lax.axis_size(axis)
+    right = [(i, (i + 1) % devices) for i in range(devices)]
+    tiles = [x]
+    while len(tiles) < devices:
+        tiles.append(lax.ppermute(tiles[-1], axis, right))
+    index = lax.axis_index(axis)
+    tiles = jnp.stack(tiles)[(index - jnp.arange(devices)) % devices]
+    return joined_along(tiles, dim)
 
 
 def from_behind(block, axis, distance):
@@ -60,7 +77,7 @@
     )
     recv_rows, recv_cot = (
         lax.all_gather(recv_rows, "tp", axis=2, tiled=True),
-        lax.all_gather(recv_cot, "tp", axis=2, tiled=True),
+        ring_gather(recv_cot, "tp", 2),
     )
     slots = groups * capacity
     routed_rows = recv_rows.reshape(slots, model_width)

time: 254 us -> 270 us (1.063)
  local copies, waits for them, and re-layouts: 2.48 us -> 15.4 us
  waiting for transfers between devices: 127 us -> 135 us
  matrix products: 34.8 us -> 29.2 us
    ppermute x0 -> x3, waiting for transfers between devices: none -> 34.2 us  [ring_gather(): tiles.append(lax.ppermute(tiles[-1], axis, right))]
    all_gather x1 -> x0, waiting for transfers between devices: 22.2 us -> none  [per_device(): lax.all_gather(recv_cot, 'tp', axis=2, tiled=True)]
    gather x0 -> x1, local copies, waits for them, and re-layouts: none -> 4.36 us  [ring_gather(): tiles = jnp.stack(tiles)[(index - jnp.arange(devices)) % devices]]
    transpose x0 -> x1, local copies, waits for them, and re-layouts: none -> 4.32 us  [joined_along(): blocks = jnp.moveaxis(blocks, 0, dim)]
    unnamed x46 -> x51, local copies, waits for them, and re-layouts: 1.45 us -> 5.69 us
    all_gather x1, waiting for transfers between devices: 3.51 us -> 0.01 us  [per_device(): lax.all_gather(recv_rows, 'tp', axis=2, tiled=True)]
    dot_general x1, matrix products: 5.69 us -> 2.31 us  [per_device(): lax.dot_general(routed_cot, down_local, contract_last, preferred_element_...]
  transfers between devices with their start and end apart: 7 -> 9, of which waited for: 6 -> 7; matrix products, arithmetic and copies ran while one was open for 9% -> 10% of each run, Pallas kernels for 0% -> 0%
where the time goes in v1:
time: 270 us
  waiting for transfers between devices  135 us (50%)
  blocking collectives  57.2 us (21%)
  matrix products  29.2 us (11%)
  local copies, waits for them, and re-layouts  15.4 us (6%)
  between operations  14.1 us (5%)
  starting transfers between devices  10.9 us (4%)
  other arithmetic  8.15 us (3%)
    reduce_scatter x1, waiting for transfers between devices, per_device(): lax.psum_scatter(lax.dot_general(stream_grad, conv_out, contract_first, p...  47.5 us
    reduce_scatter x1, waiting for transfers between devices, per_device(): lax.psum_scatter(row_partial.astype(jnp.bfloat16), 'tp', scatter_dimensio...  37 us
    ppermute x3, waiting for transfers between devices, ring_gather(): tiles.append(lax.ppermute(tiles[-1], axis, right))  34.2 us
    all_to_all x1, blocking collectives, per_device(): lax.all_to_all(sent_rows, 'sp', split_axis=0, concat_axis=0, tiled=True)  27.3 us
    all_to_all x1, blocking collectives, per_device(): lax.all_to_all(sent_cot, 'sp', split_axis=0, concat_axis=0, tiled=True)  23.2 us
    all_to_all x1, waiting for transfers between devices, per_device(): lax.all_to_all(half_grad, 'sp', split_axis=0, concat_axis=0, tiled=True)  15.2 us
    all_gather x1, blocking collectives, per_device(): moe_grad = lax.all_gather(moe_part, 'tp', axis=1, tiled=True)  6.68 us
    unnamed x51, local copies, waits for them, and re-layouts  5.69 us
  transfers between devices with their start and end apart: 9, of which 7 were waited for; matrix products, arithmetic and copies ran while one was open for 10% of the time, Pallas kernels for 0%

profile of v1, /device:TPU:0, one launch (start us, length us, event | category | flops | bytes accessed | tf_op | source)
XLA Modules:
  0.0 269.9 jit_solution(2896088067994891334)
XLA Ops:
  12.4 27.3 %all_to_all.15 = bf16[8,96,512]{2,1,0:T(8,128)(2,1)} all-to-all(bf16[8,96,512]{2,1,0:T(8,128)(2,1)S(1)} %bitcast.87), channel_id=1, replica_groups=mesh['sp'=8,'tp'=4] {'sp'}, dimensions={0} | all-to-all | bytes 1572864 | tf_op jit(solution)/shard_map/all_to_all | solution.py:75
  40.5 23.2 %all_to_all.16 = bf16[8,96,512]{2,1,0:T(8,128)(2,1)S(1)} all-to-all(bf16[8,96,512]{2,1,0:T(8,128)(2,1)S(1)} %bitcast.88), channel_id=1, replica_groups=mesh['sp'=8,'tp'=4] {'sp'}, dimensions={0} | all-to-all | bytes 1572864 | tf_op jit(solution)/shard_map/all_to_all | solution.py:76
  63.7 11.4 %collective-permute-done = bf16[8,96,512]{2,1,0:T(8,128)(2,1)S(1)} collective-permute-done((bf16[8,96,512]{2,1,0:T(8,128)(2,1)S(1)}, bf16[8,96,512]{2,1,0:T(8,128)(2,1)S(1)}, u32[]{:S(2)}, u32[]{:S(2)}) %collective-permute-start) | collective-permute-done | bytes 786464 | tf_op jit(solution)/shard_map/ppermute | solution.py:18
  75.2 11.4 %collective-permute-done.1 = bf16[8,96,512]{2,1,0:T(8,128)(2,1)S(1)} collective-permute-done((bf16[8,96,512]{2,1,0:T(8,128)(2,1)S(1)}, bf16[8,96,512]{2,1,0:T(8,128)(2,1)S(1)}, u32[]{:S(2)}, u32[]{:S(2)}) %collective-permute-start.1) | collective-permute-done | bytes 786464 | tf_op jit(solution)/shard_map/ppermute | solution.py:18
  86.6 11.4 %collective-permute-done.2 = bf16[8,96,512]{2,1,0:T(8,128)(2,1)S(1)} collective-permute-done((bf16[8,96,512]{2,1,0:T(8,128)(2,1)S(1)}, bf16[8,96,512]{2,1,0:T(8,128)(2,1)S(1)}, u32[]{:S(2)}, u32[]{:S(2)}) %collective-permute-start.2) | collective-permute-done | bytes 786464 | tf_op jit(solution)/shard_map/ppermute | solution.py:18
  98.0 1.9 pad_maximum_fusion
  99.9 4.4 %gather_fusion = bf16[4,8,96,512]{3,2,1,0:T(8,128)(2,1)} fusion(bf16[4,8,96,512]{3,2,1,0:T(8,128)(2,1)} %pad_maximum_fusion, s32[1024]{0:T(1024)S(1)} %pad_clamp_fusion), kind=kCustom, calls=%fused_computation | custom fusion | bytes 6291472 | tf_op jit(solution)/shard_map/gather | solution.py:20
  104.2 4.3 %copy.52 = bf16[8,96,4,512]{3,2,1,0:T(4,128)(2,1)S(1)} copy(bf16[8,96,4,512]{3,1,0,2:T(8,128)(2,1)} %bitcast.82) | data formatting | bytes 6291456 | tf_op jit(solution)/shard_map/transpose | solution.py:8
  108.6 2.7 copy.54
  111.3 3.8 %fusion.5 = f32[768,512]{1,0:T(8,128)S(1)} fusion(bf16[768,2048]{1,0:T(8,128)(2,1)} %bitcast.103, bf16[1,2048,512]{2,1,0:T(8,128)(2,1)S(1)} %copy-done), kind=kOutput, calls=%fused_computation.12 | convolution fusion | flops 1610612736 | bytes 6815744 | tf_op jit(solution)/shard_map/dot_general | solution.py:88
  115.1 1.8 fusion.8
  118.8 2.3 multiply_convert_fusion.1
  121.1 1.8 fusion.3
  123.0 3.5 %add_convert_fusion = bf16[768,2048]{1,0:T(8,128)(2,1)} fusion(f32[768,2048]{1,0:T(8,128)S(1)} %fusion.3, bf16[768,512]{1,0:T(8,128)(2,1)S(1)} %get-tuple-element.11, bf16[1,2048,512]{2,1,0:T(8,128)(2,1)S(1)} %copy-done.4), kind=kOutput, calls=%fused_computation.1 | convolution fusion | flops 1613758464 | bytes 12320768 | tf_op jit(solution)/shard_map/dot_general | solution.py:112
  126.6 37.0 %reduce-scatter.3.cloned.1.call-done = bf16[768,512]{1,0:T(8,128)(2,1)} async-done(((bf16[768,2048]{1,0:T(8,128)(2,1)}), bf16[768,512]{1,0:T(8,128)(2,1)}) %reduce-scatter.3.cloned.1.call-update) | async-done | bytes 786448 | tf_op jit(solution)/shard_map/reduce_scatter | solution.py:115
  163.6 5.5 %all-to-all-start.2 = ((bf16[8,96,512]{2,1,0:T(8,128)(2,1)}), bf16[8,96,512]{2,1,0:T(8,128)(2,1)S(1)}, u32[]{:S(2)}, u32[]{:S(2)}) async-start(bf16[8,96,512]{2,1,0:T(8,128)(2,1)} %bitcast.95), calls=%async_computation.3 | async-start | bytes 1572864 | tf_op jit(solution)/shard_map/all_to_all | solution.py:120
  170.0 3.9 %collective-permute-start.3 = (f32[2,256]{1,0:T(2,128)S(1)}, f32[2,256]{1,0:T(2,128)S(1)}, u32[]{:S(2)}, u32[]{:S(2)}) collective-permute-start(f32[2,256]{1,0:T(2,128)S(1)} %slice.51), channel_id=1, source_target_pairs={{0,4},{4,8},{8,12},{12,16},{16,20},{20,24},{24,28},{1,5},{5,9},{9,... | collective-permute-start | bytes 6152 | tf_op jit(solution)/shard_map/ppermute | solution.py:27
  174.0 15.2 %all-to-all-done.2 = bf16[8,96,512]{2,1,0:T(8,128)(2,1)S(1)} async-done(((bf16[8,96,512]{2,1,0:T(8,128)(2,1)}), bf16[8,96,512]{2,1,0:T(8,128)(2,1)S(1)}, u32[]{:S(2)}, u32[]{:S(2)}) %all-to-all-start.2) | async-done | bytes 786464 | tf_op jit(solution)/shard_map/all_to_all | solution.py:120
  189.5 6.7 %all_gather.7 = bf16[128,2048]{1,0:T(8,128)(2,1)S(1)} all-gather(bf16[128,512]{1,0:T(8,128)(2,1)S(1)} %fusion.14), channel_id=1, replica_groups=mesh['sp'=8,'tp'=4] {'tp'}, dimensions={1}, use_global_device_ids=true | all-gather | bytes 655360 | tf_op jit(solution)/shard_map/all_gather | solution.py:126
  198.8 5.2 %fusion = bf16[1,2048,512]{2,1,0:T(8,128)(2,1)} fusion(bf16[768,2048]{1,0:T(8,128)(2,1)} %bitcast.104, bf16[768,512]{1,0:T(8,128)(2,1)S(1)} %copy-done.9), kind=kOutput, calls=%fused_computation.6 | convolution fusion | flops 1611661312 | bytes 6029312 | tf_op jit(solution)/shard_map/dot_general | solution.py:100
  204.0 3.3 %fusion.2 = bf16[1,512,2048]{2,1,0:T(8,128)(2,1)} fusion(bf16[768,2048]{1,0:T(8,128)(2,1)S(1)} %bitcast.86, f32[768,512]{1,0:T(8,128)S(1)} %copy-done.23, f32[768,512]{1,0:T(8,128)S(1)} %copy-done.21), kind=kOutput, calls=%fused_computation.8 | convolution fusion | flops 1614020608 | bytes 8388608 | tf_op jit(solution)/shard_map/dot_general | solution.py:106
  208.8 3.2 %fusion.1 = bf16[1,2048,512]{2,1,0:T(8,128)(2,1)} fusion(bf16[768,2048]{1,0:T(8,128)(2,1)S(1)} %bitcast.106, bf16[768,512]{1,0:T(8,128)(2,1)S(1)} %copy-done.7), kind=kOutput, calls=%fused_computation.7 | convolution fusion | flops 1611661312 | bytes 6029312 | tf_op jit(solution)/shard_map/dot_general | solution.py:103
  214.3 47.5 %reduce-scatter.5.cloned.1.call-done = bf16[256,256]{1,0:T(8,128)(2,1)} async-done(((bf16[2048,256]{1,0:T(8,128)(2,1)}), bf16[256,256]{1,0:T(8,128)(2,1)}) %reduce-scatter.5.cloned.1.call-update) | async-done | bytes 131088 | tf_op jit(solution)/shard_map/reduce_scatter | solution.py:139
  261.7 1.6 convert_element_type.125
  (97 shorter events, 15.4 us)
Async XLA Ops:
  7.2 104.1 %copy-start = (bf16[1,2048,512]{2,1,0:T(8,128)(2,1)S(1)}, bf16[1,2048,512]{2,1,0:T(8,128)(2,1)}, u32[]{:S(2)}) copy-start(bf16[1,2048,512]{2,1,0:T(8,128)(2,1)} %param.16) | copy-start | bytes 6291460
  7.2 104.1 %all-gather.2.cloned.1.call-start = ((), (), s32[]{:S(2)}) async-start(), calls=%async_computation.5 | async-start | bytes 3932160 | tf_op jit(solution)/shard_map/all_gather | solution.py:79
  11.1 28.7 %copy-start.16 = (f32[128,2]{0,1:T(2,128)S(1)}, f32[128,2]{0,1:T(2,128)}, u32[]{:S(2)}) copy-start(f32[128,2]{0,1:T(2,128)} %param.15) | copy-start | bytes 3076
  11.1 29.1 %copy-start.3 = (bf16[128,2048]{1,0:T(8,128)(2,1)S(1)}, bf16[128,2048]{1,0:T(8,128)(2,1)}, u32[]{:S(2)}) copy-start(bf16[128,2048]{1,0:T(8,128)(2,1)} %param.12) | copy-start | bytes 1572868
  39.7 123.8 %reduce-scatter.3.cloned.1.call-start = ((), (), s32[]{:S(2)}) async-start(), calls=%async_computation.6 | async-start | bytes 3932160 | tf_op jit(solution)/shard_map/reduce_scatter | solution.py:115
  63.7 11.4 %collective-permute-start = (bf16[8,96,512]{2,1,0:T(8,128)(2,1)S(1)}, bf16[8,96,512]{2,1,0:T(8,128)(2,1)S(1)}, u32[]{:S(2)}, u32[]{:S(2)}) collective-permute-start(bf16[8,96,512]{2,1,0:T(8,128)(2,1)S(1)} %all_to_all.16), channel_id=1, source_target_pairs={{0,1},{1,2},{2,3},{3,0},{4,5},{5,6},{6,7},{7,4},{8,9},{9,10},{10,1... | collective-permute-start | bytes 2359304 | tf_op jit(solution)/shard_map/ppermute | solution.py:18
  75.2 11.4 %collective-permute-start.1 = (bf16[8,96,512]{2,1,0:T(8,128)(2,1)S(1)}, bf16[8,96,512]{2,1,0:T(8,128)(2,1)S(1)}, u32[]{:S(2)}, u32[]{:S(2)}) collective-permute-start(bf16[8,96,512]{2,1,0:T(8,128)(2,1)S(1)} %collective-permute-done), channel_id=1, source_target_pairs={{0,1},{1,2},{2,3},{3,0},{4,5},{5,6},{6,7},{7,4},{8,9},{9,10},{10,1... | collective-permute-start | bytes 2359304 | tf_op jit(solution)/shard_map/ppermute | solution.py:18
  86.6 11.4 %collective-permute-start.2 = (bf16[8,96,512]{2,1,0:T(8,128)(2,1)S(1)}, bf16[8,96,512]{2,1,0:T(8,128)(2,1)S(1)}, u32[]{:S(2)}, u32[]{:S(2)}) collective-permute-start(bf16[8,96,512]{2,1,0:T(8,128)(2,1)S(1)} %collective-permute-done.1), channel_id=1, source_target_pairs={{0,1},{1,2},{2,3},{3,0},{4,5},{5,6},{6,7},{7,4},{8,9},{9,10},{10,1... | collective-permute-start | bytes 2359304 | tf_op jit(solution)/shard_map/ppermute | solution.py:18
  116.9 4.2 %copy-start.22 = (f32[768,512]{1,0:T(8,128)}, f32[768,512]{1,0:T(8,128)S(1)}, u32[]{:S(2)}) copy-start(f32[768,512]{1,0:T(8,128)S(1)} %fusion.8) | copy-start | bytes 4718596
  126.5 47.4 %copy-start.15 = (bf16[3,256]{1,0:T(4,128)(2,1)S(1)}, bf16[3,256]{1,0:T(4,128)(2,1)}, u32[]{:S(2)}) copy-start(bf16[3,256]{1,0:T(4,128)(2,1)} %param.22) | copy-start | bytes 4612
  163.6 25.6 %all-to-all-start.2 = ((bf16[8,96,512]{2,1,0:T(8,128)(2,1)}), bf16[8,96,512]{2,1,0:T(8,128)(2,1)S(1)}, u32[]{:S(2)}, u32[]{:S(2)}) async-start(bf16[8,96,512]{2,1,0:T(8,128)(2,1)} %bitcast.95), calls=%async_computation.3 | async-start | bytes 1572864 | tf_op jit(solution)/shard_map/all_to_all | solution.py:120
  169.1 92.6 %reduce-scatter.5.cloned.1.call-start = ((), (), s32[]{:S(2)}) async-start(), calls=%async_computation.7 | async-start | bytes 1179648 | tf_op jit(solution)/shard_map/reduce_scatter | solution.py:139
  170.0 26.2 %collective-permute-start.3 = (f32[2,256]{1,0:T(2,128)S(1)}, f32[2,256]{1,0:T(2,128)S(1)}, u32[]{:S(2)}, u32[]{:S(2)}) collective-permute-start(f32[2,256]{1,0:T(2,128)S(1)} %slice.51), channel_id=1, source_target_pairs={{0,4},{4,8},{8,12},{12,16},{16,20},{20,24},{24,28},{1,5},{5,9},{9,... | collective-permute-start | bytes 6152 | tf_op jit(solution)/shard_map/ppermute | solution.py:27
  189.2 7.1 %copy-start.5 = (bf16[2048,256]{1,0:T(8,128)(2,1)S(1)}, bf16[2048,256]{1,0:T(8,128)(2,1)}, u32[]{:S(2)}) copy-start(bf16[2048,256]{1,0:T(8,128)(2,1)} %param.23) | copy-start | bytes 3145732
  189.2 7.1 %copy-start.11 = (f32[128,256]{1,0:T(8,128)S(1)}, f32[128,256]{1,0:T(8,128)}, u32[]{:S(2)}) copy-start(f32[128,256]{1,0:T(8,128)} %copy-done.10) | copy-start | bytes 393220
  189.2 7.1 %copy-start.12 = (bf16[128,256]{1,0:T(8,128)(2,1)S(1)}, bf16[128,256]{1,0:T(8,128)(2,1)}, u32[]{:S(2)}) copy-start(bf16[128,256]{1,0:T(8,128)(2,1)} %param.19) | copy-start | bytes 196612
  198.7 5.2 %copy-start.2 = (bf16[96,8,4,512]{3,1,2,0:T(8,128)(2,1)S(1)}, bf16[96,8,4,512]{3,1,2,0:T(8,128)(2,1)}, u32[]{:S(2)}) copy-start(bf16[96,8,4,512]{3,1,2,0:T(8,128)(2,1)} %copy.54) | copy-start | bytes 9437188
  198.7 5.2 %copy-start.21 = (f32[768,512]{1,0:T(8,128)S(1)}, f32[768,512]{1,0:T(8,128)}, u32[]{:S(2)}) copy-start(f32[768,512]{1,0:T(8,128)} %copy-done.20) | copy-start | bytes 4718596
  198.7 5.2 %copy-start.23 = (f32[768,512]{1,0:T(8,128)S(1)}, f32[768,512]{1,0:T(8,128)}, u32[]{:S(2)}) copy-start(f32[768,512]{1,0:T(8,128)} %copy-done.22) | copy-start | bytes 4718596
  204.0 4.8 %copy-start.7 = (bf16[768,512]{1,0:T(8,128)(2,1)S(1)}, bf16[768,512]{1,0:T(8,128)(2,1)}, u32[]{:S(2)}) copy-start(bf16[768,512]{1,0:T(8,128)(2,1)} %copy-done.6) | copy-start | bytes 2359300
  204.0 4.8 %copy-start.18 = (bf16[8,96,2048]{2,1,0:T(8,128)(2,1)S(1)}, bf16[8,96,2048]{2,1,0:T(8,128)(2,1)}, u32[]{:S(2)}) copy-start(bf16[8,96,2048]{2,1,0:T(8,128)(2,1)} %all-gather.2.cloned.1.call-done) | copy-start | bytes 9437188
  207.3 5.6 %copy-start.13 = (bf16[128,256]{1,0:T(8,128)(2,1)S(1)}, bf16[128,256]{1,0:T(8,128)(2,1)}, u32[]{:S(2)}) copy-start(bf16[128,256]{1,0:T(8,128)(2,1)} %param.20) | copy-start | bytes 196612
  207.3 6.3 %copy-start.14 = (bf16[128,256]{1,0:T(8,128)(2,1)S(1)}, bf16[128,256]{1,0:T(8,128)(2,1)}, u32[]{:S(2)}) copy-start(bf16[128,256]{1,0:T(8,128)(2,1)} %param.21) | copy-start | bytes 196612
  207.3 5.6 %collective-permute-start.4 = (f32[2,256]{1,0:T(2,128)S(1)}, f32[2,256]{1,0:T(2,128)S(1)}, u32[]{:S(2)}, u32[]{:S(2)}) collective-permute-start(f32[2,256]{1,0:T(2,128)S(1)} %slice.56), channel_id=1, source_target_pairs={{4,0},{8,4},{12,8},{16,12},{20,16},{24,20},{28,24},{5,1},{9,5},{13... | collective-permute-start | bytes 6152 | tf_op jit(solution)/shard_map/ppermute | solution.py:27
  (9 other events, 24.8 us)
Sparse Core Ops, SparseCore 0:
  39.9 27.5 all-gather.1
  126.7 36.8 reduce-scatter.2
  198.8 62.8 reduce-scatter.4
